TPU v7x, 32 devices: a whole 2x2x4 slice. The times are simulated.
32 devices in a mesh: sp: 4 (over y, x), tp: 8 (over z, core).
Axes of the slice: x: 2, y: 2, z: 4, core: 2. Of those that a mesh axis runs over, the one named last changes fastest.
Arguments:
- queries: bfloat16 [1536, 2048], P('sp', 'tp'), may hold values from -6 to 6
- keys: bfloat16 [1536, 2048], P('sp', 'tp'), may hold values from -6 to 6
- values: bfloat16 [1536, 2048], P('sp', 'tp'), may hold values from -6 to 6
- key_bias: bfloat16 [1536, 32], P('sp', 'tp'), may hold values from -16 to 0
- head_gain: float32 [32, 64], P('tp'), may hold values from 0.1 to 1.9
- out_weight: bfloat16 [2048, 2048], P('tp'), may hold values from -0.125 to 0.125
- residual: bfloat16 [1536, 2048], P(('sp', 'tp')), may hold values from -6 to 6
- norm_gain: float32 [2048], replicated, may hold values from 0.1 to 1.9
- gate_proj: bfloat16 [4, 2048, 7168], P('sp', None, 'tp'), may hold values from -0.125 to 0.125
- up_proj: bfloat16 [4, 2048, 7168], P('sp', None, 'tp'), may hold values from -0.125 to 0.125
- down_proj: bfloat16 [4, 7168, 2048], P('sp', 'tp'), may hold values from -0.0625 to 0.0625
- expert_choice: int32 [1536, 2], P(('sp', 'tp')), may hold values from 0 to 3, all different within a row; in each aligned block of 48 rows (0 to 47, 48 to 95, ...) at most 48 rows name the same one
- expert_weights: float32 [1536, 2], P(('sp', 'tp')), may hold values from 0.2 to 1
Outputs:
- layer_out: bfloat16 [1536, 2048], P(('sp', 'tp'))
Inputs may be any that keep to these rules, and one draw needn't show every extreme that they name: `expert_choice`: in each aligned block of 48 rows (the rows of one device), no expert is named more than 48 times; the two experts of a row differ.
All inputs are finite; a program needn't handle non-finite values.
Results may differ from a plain program's by a relative error of at most 0.019.
Values may be sent and summed in bfloat16 or wider, within the bound.
A program may use at most 128 MiB of HBM per device.

v0:
```python
import jax
import jax.numpy as jnp
from jax import lax
from jax.sharding import PartitionSpec as P

epsilon = 1e-06


def rms_scaled(values_in):
    return values_in * lax.rsqrt(jnp.mean(values_in * values_in, axis=-1, keepdims=True) + epsilon)


def expert_partial(row_block, gate_matrix, up_matrix, down_matrix):
    gate_part = jnp.dot(row_block, gate_matrix, preferred_element_type=jnp.float32)
    up_part = jnp.dot(row_block, up_matrix, preferred_element_type=jnp.float32)
    hidden = (jax.nn.silu(gate_part) * up_part).astype(jnp.bfloat16)
    return jnp.dot(hidden, down_matrix, preferred_element_type=jnp.float32)


def choice_ranks(routes, experts_all):
    flat_routes = routes.reshape(routes.shape[:-2] + (-1,))
    onehot = (flat_routes[..., None] == jnp.arange(experts_all, dtype=jnp.int32)).astype(jnp.int32)
    before = jnp.cumsum(onehot, axis=-2) - onehot
    return jnp.sum(before * onehot, axis=-1).reshape(routes.shape)


def slot_tokens(slot_index, targets, missing):
    flat_slots = slot_index.reshape(-1)
    owners = jnp.arange(flat_slots.shape[0], dtype=jnp.int32) // 2
    matches = flat_slots[None, :] == jnp.arange(targets, dtype=jnp.int32)[:, None]
    owner_found = jnp.sum(jnp.where(matches, owners[None, :], 0), axis=1)
    return jnp.where(jnp.any(matches, axis=1), owner_found, missing)


def on_device(
    queries,
    keys,
    values,
    key_bias,
    head_gain,
    out_weight,
    residual,
    norm_gain,
    gate_proj,
    up_proj,
    down_proj,
    expert_choice,
    expert_weights,
):
    rows_own = queries.shape[0]
    heads_here = head_gain.shape[0]
    head_size = head_gain.shape[1]
    model_width = out_weight.shape[1]
    seq_devices = lax.axis_size("sp")
    head_devices = lax.axis_size("tp")
    own_start = lax.axis_index("sp") * rows_own
    query_pos = own_start + jnp.arange(rows_own, dtype=jnp.int32)
    query_heads = queries.reshape(rows_own, heads_here, head_size)

    def key_block(slot_state, key_rows, value_rows, bias_rows, key_start):
        key_heads = key_rows.reshape(rows_own, heads_here, head_size)
        value_heads = value_rows.reshape(rows_own, heads_here, head_size)
        scores = jnp.einsum(
            "qhd,khd->hqk", query_heads, key_heads, preferred_element_type=jnp.float32
        ) * head_size ** (-0.5)
        scores = scores + bias_rows.astype(jnp.float32).T[:, None, :]
        key_pos = key_start + jnp.arange(rows_own, dtype=jnp.int32)
        earlier = (key_pos[None, :] < query_pos[:, None])[None, :, :]
        log_drops = jnp.where(earlier, jax.nn.log_sigmoid(-scores), 0.0)
        suffix = lax.cumsum(log_drops, axis=2, reverse=True) - log_drops
        within = jnp.where(earlier, jnp.exp(jax.nn.log_sigmoid(scores) + suffix), 0.0).astype(
            jnp.bfloat16
        )
        block_part = jnp.einsum(
            "hqk,khd->qhd", within, value_heads, preferred_element_type=jnp.float32
        )
        block_index = key_start // rows_own
        sums_new = lax.dynamic_update_index_in_dim(
            slot_state[0], block_part.reshape(rows_own, heads_here * head_size), block_index, 0
        )
        totals_new = lax.dynamic_update_index_in_dim(
            slot_state[1], jnp.sum(log_drops, axis=2), block_index, 0
        )
        return (sums_new, totals_new)

    empty_state = (
        jnp.zeros((seq_devices, rows_own, heads_here * head_size), jnp.float32),
        jnp.zeros((seq_devices, heads_here, rows_own), jnp.float32),
    )
    key_piece = lax.all_gather(keys, "sp", axis=0, tiled=True)
    value_piece = lax.all_gather(values, "sp", axis=0, tiled=True)
    bias_piece = lax.all_gather(key_bias, "sp", axis=0, tiled=True)

    def visit(block_count, state_in):
        offset = block_count * rows_own

        def take_rows(array):
            return lax.dynamic_slice_in_dim(array, offset, rows_own, 0)

        def compute(state_now):
            return key_block(
                state_now,
                take_rows(key_piece),
                take_rows(value_piece),
                take_rows(bias_piece),
                offset,
            )

        def keep(state_now):
            return state_now

        return lax.cond(offset <= own_start, compute, keep, state_in)

    block_sums, totals = lax.fori_loop(0, key_piece.shape[0] // rows_own, visit, empty_state)
    carried = jnp.sum(totals, axis=0, keepdims=True) - jnp.cumsum(totals, axis=0)
    factors = jnp.exp(carried).transpose(0, 2, 1)[..., None]
    mixture = jnp.sum(
        factors * block_sums.reshape(seq_devices, rows_own, heads_here, head_size), axis=0
    )
    attended = (
        (rms_scaled(mixture) * head_gain)
        .astype(jnp.bfloat16)
        .reshape(rows_own, heads_here * head_size)
    )
    row_share = rows_own // head_devices
    merged = lax.all_to_all(attended, "tp", split_axis=0, concat_axis=1, tiled=True)
    projected = jnp.dot(
        merged,
        lax.all_gather(out_weight, "tp", axis=0, tiled=True),
        preferred_element_type=jnp.float32,
    )
    stream = (residual.astype(jnp.float32) + projected).astype(jnp.bfloat16)
    normed = (rms_scaled(stream.astype(jnp.float32)) * norm_gain).astype(jnp.bfloat16)
    local_experts = gate_proj.shape[0]
    experts_all = local_experts * seq_devices
    capacity = 4 * rows_own // (head_devices * experts_all)
    own_slots = expert_choice * capacity + choice_ranks(expert_choice, experts_all)
    wanted = slot_tokens(own_slots, experts_all * capacity, row_share)
    outgoing = jnp.take(normed, wanted, axis=0, mode="fill", fill_value=0)
    arrived = lax.all_to_all(
        outgoing.reshape(seq_devices, local_experts, capacity, model_width),
        "sp",
        split_axis=0,
        concat_axis=0,
        tiled=True,
    )
    row_piece = lax.all_gather(arrived, "tp", axis=0, tiled=True)
    count_rows = row_piece.shape[0]
    partials = jnp.stack(
        [
            expert_partial(
                row_piece[:, 0].reshape(-1, model_width), gate_proj[0], up_proj[0], down_proj[0]
            ).reshape(count_rows, capacity, model_width)
        ],
        axis=1,
    )
    summed = lax.psum_scatter(partials.astype(jnp.bfloat16), "tp", scatter_dimension=0, tiled=True)
    returned = lax.all_to_all(summed, "sp", split_axis=0, concat_axis=0, tiled=True).reshape(
        experts_all * capacity, model_width
    )
    picked = jnp.take(returned, own_slots, axis=0).astype(jnp.float32)
    combined = jnp.sum(expert_weights[:, :, None] * picked, axis=1)
    return (stream.astype(jnp.float32) + combined).astype(jnp.bfloat16)


def solution(mesh):
    placed = (
        P("sp", "tp"),
        P("sp", "tp"),
        P("sp", "tp"),
        P("sp", "tp"),
        P("tp", None),
        P("tp", None),
        P(("sp", "tp"), None),
        P(),
        P("sp", None, "tp"),
        P("sp", None, "tp"),
        P("sp", "tp", None),
        P(("sp", "tp"), None),
        P(("sp", "tp"), None),
    )
    return jax.shard_map(
        on_device, mesh=mesh, in_specs=placed, out_specs=P(("sp", "tp"), None), check_vma=False
    )
```

profile of v0, /device:TPU:0, one launch (start us, length us, event | category | flops | bytes accessed | tf_op | source)
XLA Modules:
  0.0 380.5 jit_solution(13210839301603181166)
XLA Ops:
  9.4 1.7 copy.83
  11.2 11.0 %all_gather.17 = bf16[1536,4]{0,1:T(4,128)(2,1)} all-gather(bf16[384,4]{0,1:T(4,128)(2,1)} %param.20), channel_id=1, replica_groups=mesh['sp'=4,'tp'=8] {'sp'}, dimensions={0}, use_global_device_ids=true | all-gather | bytes 15360 | tf_op jit(solution)/shard_map/all_gather | solution.py:92
  22.2 12.4 %all_gather.15 = bf16[1536,256]{0,1:T(8,128)(2,1)} all-gather(bf16[384,256]{0,1:T(8,128)(2,1)S(1)} %copy.81), channel_id=1, replica_groups=mesh['sp'=4,'tp'=8] {'sp'}, dimensions={0}, use_global_device_ids=true | all-gather | bytes 983040 | tf_op jit(solution)/shard_map/all_gather | solution.py:91
  34.5 13.4 %all_gather.16 = bf16[1536,256]{0,1:T(8,128)(2,1)} all-gather(bf16[384,256]{0,1:T(8,128)(2,1)S(1)} %copy.82), channel_id=1, replica_groups=mesh['sp'=4,'tp'=8] {'sp'}, dimensions={0}, use_global_device_ids=true | all-gather | bytes 983040 | tf_op jit(solution)/shard_map/all_gather | solution.py:90
  47.9 1.3 broadcast_in_dim.84
  49.8 28.2 %while.17 = (s32[]{:T(128)}, f32[4,384,256]{1,2,0:T(8,128)}, f32[4,4,384]{2,1,0:T(4,128)}, s32[]{:T(128)}, bf16[1536,256]{0,1:T(8,128)(2,1)}, /*index=5*/bf16[15...) while((s32[]{:T(128)}, f32[4,384,256]{1,2,0:T(8,128)}, ...), condition=%wide.region_6.7_spmd.clone.clone, body=%wide.region_0.6_spmd.clone.clone.sunk | while | flops 246117120 | bytes 38572464 | solution.py:114
  49.8 28.0 %conditional.4 = ((f32[4,384,256]{1,2,0:T(8,128)}, f32[4,4,384]{2,1,0:T(4,128)})) conditional(s32[]{:T(128)} %convert_element_type.76, (f32[4,384,256]{1,2,0:T(8,128)}, f32[4,4,384]{2,1,0:T(4,128)}) %tuple.53, (s32[]{:T(128)}, bf16[1536,256]{0,1:T(8,128)(2,1)}, s32[]{:T(128)}, bf16[1536,256]{0,1:T(8,128)(2,1)}, bf16[384,4,64]{0,2,1:T(8,128)(2,1)}, ...), branch_computations={%region_1.0_spmd, %region_2.5_spmd} | conditional | flops 246117120 | bytes 38570716 | solution.py:112
  51.7 4.3 %fusion.15 = (f32[4,384]{1,0:T(4,128)S(1)}, f32[4,384,384]{1,2,0:T(8,128)S(1)}, f32[4,384,384]{2,1,0:T(8,128)}) fusion(f32[4,384]{1,0:T(4,128)S(1)} %convert_bitcast_fusion, pred[384,384]{0,1:T(8,128)(4,1)S(1)} %broadcast_compare_fusion, bf16[384,4,64]{0,2,1:T(8,128)(2,1)S(1)} %bitcast.92, bf16[384,4,64]{0,2,1:T(8,128)(2,1)} %get-tuple-element.177), kind=kOutput, calls=%fused_computation.33 | convolution fusion | flops 81984000 | bytes 5271552 | tf_op jit(solution)/shard_map/while/body/eval_jaxpr/cond/branch_1_fun/qhd,khd->hqk/dot_general | solution.py:63
  56.0 14.0 %fusion.2 = f32[4,384,3,128]{1,2,3,0:T(4,128)S(1)} fusion(f32[4,384,3,128]{1,3,2,0:T(8,128)S(1)} %bitcast.88), kind=kOutput, calls=%fused_computation.5 | output fusion | flops 74907648 | bytes 4718592 | tf_op jit(solution)/shard_map/reduce-window
  70.9 1.5 copy-done
  72.3 3.6 fusion.8
  79.5 1.6 fusion.22
  83.2 4.8 %all-to-all-start = ((bf16[8,48,256]{2,1,0:T(8,128)(2,1)}), bf16[8,48,256]{2,1,0:T(8,128)(2,1)S(1)}, u32[]{:S(2)}, u32[]{:S(2)}) async-start(bf16[8,48,256]{2,1,0:T(8,128)(2,1)} %multiply_convert_fusion.2), calls=%async_computation | async-start | bytes 393216 | tf_op jit(solution)/shard_map/all_to_all | solution.py:126
  89.5 6.8 %all-to-all-done = bf16[8,48,256]{2,1,0:T(8,128)(2,1)S(1)} async-done(((bf16[8,48,256]{2,1,0:T(8,128)(2,1)}), bf16[8,48,256]{2,1,0:T(8,128)(2,1)S(1)}, u32[]{:S(2)}, u32[]{:S(2)}) %all-to-all-start) | async-done | bytes 196640 | tf_op jit(solution)/shard_map/all_to_all | solution.py:126
  96.4 5.1 %multiply_reduce_fusion.1 = (f32[48]{0:T(128)S(1)}, f32[48,2048]{1,0:T(8,128)S(1)}) fusion(bf16[48,2048]{1,0:T(8,128)(2,1)S(1)} %bitcast.94, bf16[2048,2048]{1,0:T(8,128)(2,1)} %all-gather.3.cloned.1.call-done, bf16[48,2048]{1,0:T(8,128)(2,1)S(1)} %copy-done.1), kind=kOutput, calls=%fused_computation.54 | convolution fusion | flops 403242944 | bytes 9175232 | tf_op jit(solution)/shard_map/dot_general | solution.py:127
  102.9 96.4 %all_to_all.26 = bf16[4,1,48,2048]{3,2,1,0:T(8,128)(2,1)} all-to-all(bf16[4,1,48,2048]{3,2,1,0:T(8,128)(2,1)S(1)} %broadcast_select_fusion), channel_id=1, replica_groups=mesh['sp'=4,'tp'=8] {'sp'}, dimensions={0} | all-to-all | bytes 1572864 | tf_op jit(solution)/shard_map/all_to_all | solution.py:140
  199.4 63.5 %all-gather.5.cloned.1.call-done = bf16[32,1,48,2048]{3,2,1,0:T(8,128)(2,1)} async-done(((bf16[4,1,48,2048]{3,2,1,0:T(8,128)(2,1)}), bf16[32,1,48,2048]{3,2,1,0:T(8,128)(2,1)}) %all-gather.5.cloned.1.call-update) | async-done | bytes 6291472 | tf_op jit(solution)/shard_map/all_gather | solution.py:147
  262.9 10.0 %fusion.18 = f32[1536,896]{1,0:T(8,128)S(1)} fusion(bf16[1536,2048]{1,0:T(8,128)(2,1)} %bitcast.101, bf16[1,2048,896]{2,1,0:T(8,128)(2,1)} %param.25), kind=kOutput, calls=%fused_computation.38 | convolution fusion | flops 5637144576 | bytes 15466496 | tf_op jit(solution)/shard_map/dot_general | solution.py:14
  272.9 7.1 %multiply_convert_fusion = bf16[1536,896]{1,0:T(8,128)(2,1)S(1)} fusion(f32[1536,896]{1,0:T(8,128)S(1)} %fusion.18, bf16[1536,2048]{1,0:T(8,128)(2,1)S(1)} %bitcast.102, bf16[1,2048,896]{2,1,0:T(8,128)(2,1)S(1)} %copy-done.7), kind=kOutput, calls=%fused_computation.35 | convolution fusion | flops 5645402112 | bytes 18219008 | tf_op jit(solution)/shard_map/dot_general | solution.py:15
  280.0 8.7 %convert_bitcast_fusion.1 = bf16[32,1,48,2048]{3,2,0,1:T(8,128)(2,1)} fusion(bf16[32,48,896]{2,1,0:T(8,128)(2,1)S(1)} %bitcast.103, bf16[1,896,2048]{2,1,0:T(8,128)(2,1)S(1)} %copy-done.8), kind=kOutput, calls=%fused_computation.34 | convolution fusion | flops 5640290304 | bytes 12713984 | tf_op jit(solution)/shard_map/dot_general | solution.py:17
  288.8 68.5 %reduce-scatter.2.cloned.1.call-done = bf16[4,1,48,2048]{3,2,0,1:T(8,128)(2,1)} async-done(((bf16[32,1,48,2048]{3,2,0,1:T(8,128)(2,1)}), bf16[4,1,48,2048]{3,2,0,1:T(8,128)(2,1)}) %reduce-scatter.2.cloned.1.call-update) | async-done | bytes 786448 | tf_op jit(solution)/shard_map/reduce_scatter | solution.py:157
  357.3 3.7 all-to-all-start.2
  361.5 8.6 %all-to-all-done.2 = bf16[4,1,48,2048]{3,2,1,0:T(8,128)(2,1)S(1)} async-done(((bf16[4,1,48,2048]{3,2,1,0:T(8,128)(2,1)}), bf16[4,1,48,2048]{3,2,1,0:T(8,128)(2,1)S(1)}, u32[]{:S(2)}, u32[]{:S(2)}) %all-to-all-start.2) | async-done | bytes 786464 | tf_op jit(solution)/shard_map/all_to_all | solution.py:158
  371.2 2.1 multiply_reduce_fusion
  (88 shorter events, 16.8 us)
Async XLA Ops:
  6.5 89.9 %all-gather.3.cloned.1.call-start = ((), (), s32[]{:S(2)}) async-start(), calls=%async_computation.4 | async-start | bytes 9437184 | tf_op jit(solution)/shard_map/all_gather | solution.py:129
  70.6 1.7 copy-start
  79.5 2.9 copy-start.4
  81.1 7.0 %copy-start.3 = (s32[48,2]{0,1:T(2,128)S(1)}, s32[48,2]{0,1:T(2,128)}, u32[]{:S(2)}) copy-start(s32[48,2]{0,1:T(2,128)} %param.28) | copy-start | bytes 1156
  81.3 15.1 %copy-start.1 = (bf16[48,2048]{1,0:T(8,128)(2,1)S(1)}, bf16[48,2048]{1,0:T(8,128)(2,1)}, u32[]{:S(2)}) copy-start(bf16[48,2048]{1,0:T(8,128)(2,1)} %param.23) | copy-start | bytes 589828
  83.2 13.1 %all-to-all-start = ((bf16[8,48,256]{2,1,0:T(8,128)(2,1)}), bf16[8,48,256]{2,1,0:T(8,128)(2,1)S(1)}, u32[]{:S(2)}, u32[]{:S(2)}) async-start(bf16[8,48,256]{2,1,0:T(8,128)(2,1)} %multiply_convert_fusion.2), calls=%async_computation | async-start | bytes 393216 | tf_op jit(solution)/shard_map/all_to_all | solution.py:126
  88.0 174.9 %all-gather.5.cloned.1.call-start = ((), (), s32[]{:S(2)}) async-start(), calls=%async_computation.5 | async-start | bytes 7077888 | tf_op jit(solution)/shard_map/all_gather | solution.py:147
  96.4 5.1 %copy-start.2 = (f32[2048]{0:T(1024)S(1)}, f32[2048]{0:T(1024)}, u32[]{:S(2)}) copy-start(f32[2048]{0:T(1024)} %param.24) | copy-start | bytes 24580
  199.3 158.0 %reduce-scatter.2.cloned.1.call-start = ((), (), s32[]{:S(2)}) async-start(), calls=%async_computation.6 | async-start | bytes 7077888 | tf_op jit(solution)/shard_map/reduce_scatter | solution.py:157
  262.9 10.0 %copy-start.6 = (bf16[32,1,48,2048]{3,2,1,0:T(8,128)(2,1)S(1)}, bf16[32,1,48,2048]{3,2,1,0:T(8,128)(2,1)}, u32[]{:S(2)}) copy-start(bf16[32,1,48,2048]{3,2,1,0:T(8,128)(2,1)} %all-gather.5.cloned.1.call-done) | copy-start | bytes 18874372
  262.9 10.0 %copy-start.7 = (bf16[1,2048,896]{2,1,0:T(8,128)(2,1)S(1)}, bf16[1,2048,896]{2,1,0:T(8,128)(2,1)}, u32[]{:S(2)}) copy-start(bf16[1,2048,896]{2,1,0:T(8,128)(2,1)} %param.26) | copy-start | bytes 11010052
  272.9 7.1 %copy-start.8 = (bf16[1,896,2048]{2,1,0:T(8,128)(2,1)S(1)}, bf16[1,896,2048]{2,1,0:T(8,128)(2,1)}, u32[]{:S(2)}) copy-start(bf16[1,896,2048]{2,1,0:T(8,128)(2,1)} %param.27) | copy-start | bytes 11010052
  288.8 72.6 %copy-start.5 = (f32[48,2]{0,1:T(2,128)S(1)}, f32[48,2]{0,1:T(2,128)}, u32[]{:S(2)}) copy-start(f32[48,2]{0,1:T(2,128)} %param.29) | copy-start | bytes 1156
  357.3 12.7 %all-to-all-start.2 = ((bf16[4,1,48,2048]{3,2,1,0:T(8,128)(2,1)}), bf16[4,1,48,2048]{3,2,1,0:T(8,128)(2,1)S(1)}, u32[]{:S(2)}, u32[]{:S(2)}) async-start(bf16[4,1,48,2048]{3,2,1,0:T(8,128)(2,1)} %bitcast.96), calls=%async_computation.3 | async-start | bytes 1572864 | tf_op jit(solution)/shard_map/all_to_all | solution.py:158
Sparse Core Ops, SparseCore 0:
  8.9 84.8 all-gather.2
  199.4 63.4 all-gather.4
  288.9 68.3 reduce-scatter.1
where the time goes:
time: 382 us; the launch traced here: 380 us
  waiting for transfers between devices  148 us (39%)
  blocking collectives  133 us (35%)
  matrix products  35.5 us (9%)
  other arithmetic  26.7 us (7%)
  local copies, waits for them, and re-layouts  14.7 us (4%)
  between operations  13.4 us (4%)
  starting transfers between devices  8.62 us (2%)
    all_to_all x1, blocking collectives, on_device(): lax.all_to_all(outgoing.reshape(seq_devices, local_experts, capacity, mod...  96.4 us
    reduce_scatter x1, waiting for transfers between devices, on_device(): lax.psum_scatter(partials.astype(jnp.bfloat16), 'tp', scatter_dimension=0...  68.5 us
    all_gather x1, waiting for transfers between devices, on_device(): row_piece = lax.all_gather(arrived, 'tp', axis=0, tiled=True)  63.5 us
    another operation x2, other arithmetic  14.1 us
    all_gather x1, blocking collectives, on_device(): key_piece = lax.all_gather(keys, 'sp', axis=0, tiled=True)  13.4 us
    all_gather x1, blocking collectives, on_device(): value_piece = lax.all_gather(values, 'sp', axis=0, tiled=True)  12.4 us
    all_gather x1, blocking collectives, on_device(): bias_piece = lax.all_gather(key_bias, 'sp', axis=0, tiled=True)  11 us
    dot_general x1, matrix products, expert_partial(): jnp.dot(row_block, gate_matrix, preferred_element_type=jnp.float32)  9.96 us
  transfers between devices with their start and end apart: 5, of which 4 were waited for; matrix products, arithmetic and copies ran while one was open for 10% of the time, Pallas kernels for 0%

commit v1 on v0

--- a/solution.py
+++ b/solution.py
@@ -4,6 +4,35 @@
 from jax.sharding import PartitionSpec as P
 
 epsilon = 1e-06
+
+
+def expand_cycles(z_in, array_dim, vector):
+    y2, seen_now = (z_in.shape[:array_dim], z_in.shape[array_dim + 1 :])
+    block_last = z_in.reshape(*y2, vector, -1, *seen_now)
+    return jnp.moveaxis(block_last, array_dim, 0)
+
+
+def test_the_sections(patch, axis_k):
+    local_next = list(patch.shape[1:])
+    local_next[axis_k] *= patch.shape[0]
+    return jnp.moveaxis(patch, 0, axis_k).reshape(local_next)
+
+
+def tell_the_rates(x_local, bus_axis, local_values, vec):
+    lower = jax.lax.psum(1, bus_axis)
+    r2 = jax.lax.axis_index(bus_axis)
+    p_next, f_now = (lower, r2)
+    field_out = expand_cycles(x_local, local_values, p_next)
+    pieces_in = [field_out[f_now]]
+    for i0 in [*range(1, p_next)]:
+        arr_out = field_out[(f_now + i0) % p_next]
+        v_now = jax.lax.ppermute(
+            arr_out, bus_axis, [(at, (at + i0) % p_next) for at in range(p_next)]
+        )
+        pieces_in.append(v_now)
+    f_next = jnp.stack(pieces_in, axis=0)
+    field_out = f_next[(f_now - jnp.arange(p_next)) % p_next]
+    return test_the_sections(field_out, vec)
 
 
 def rms_scaled(values_in):
@@ -137,12 +166,8 @@
     own_slots = expert_choice * capacity + choice_ranks(expert_choice, experts_all)
     wanted = slot_tokens(own_slots, experts_all * capacity, row_share)
     outgoing = jnp.take(normed, wanted, axis=0, mode="fill", fill_value=0)
-    arrived = lax.all_to_all(
-        outgoing.reshape(seq_devices, local_experts, capacity, model_width),
-        "sp",
-        split_axis=0,
-        concat_axis=0,
-        tiled=True,
+    arrived = tell_the_rates(
+        outgoing.reshape(seq_devices, local_experts, capacity, model_width), "sp", 0, 0
     )
     row_piece = lax.all_gather(arrived, "tp", axis=0, tiled=True)
     count_rows = row_piece.shape[0]

time: 382 us -> 390 us (1.021)
  blocking collectives: 133 us -> 36.7 us
  starting transfers between devices: 8.62 us -> 94.3 us
  waiting for transfers between devices: 148 us -> 157 us
  loops' own time: 0.31 us -> 8.81 us
    all_to_all x1 -> x0, blocking collectives: 96.4 us -> none  [on_device(): lax.all_to_all(outgoing.reshape(seq_devices, local_experts, capacity, mod...]
    ppermute x0 -> x3, starting transfers between devices: none -> 85.6 us  [tell_the_rates(): jax.lax.ppermute(arr_out, bus_axis, [(at, (at + i0) % p_next) for at in r...]
    another operation x1, loops' own time: 0.2 us -> 8.7 us  [on_device(): lax.fori_loop(0, key_piece.shape[0] // rows_own, visit, empty_state)]
    ppermute x0 -> x3, waiting for transfers between devices: none -> 7.42 us  [tell_the_rates(): jax.lax.ppermute(arr_out, bus_axis, [(at, (at + i0) % p_next) for at in r...]
    another operation x2 -> x3, other arithmetic: 14.1 us -> 14.2 us
  transfers between devices with their start and end apart: 5 -> 8, of which waited for: 4 -> 6; matrix products, arithmetic and copies ran while one was open for 10% -> 10% of each run, Pallas kernels for 0% -> 0%
where the time goes in v1:
time: 390 us; the launch traced here: 389 us
  waiting for transfers between devices  157 us (40%)
  starting transfers between devices  94.3 us (24%)
  blocking collectives  36.7 us (9%)
  matrix products  35.5 us (9%)
  other arithmetic  26.8 us (7%)
  local copies, waits for them, and re-layouts  16.3 us (4%)
  between operations  13.8 us (4%)
  loops' own time  8.81 us (2%)
    ppermute x3, starting transfers between devices, tell_the_rates(): jax.lax.ppermute(arr_out, bus_axis, [(at, (at + i0) % p_next) for at in r...  85.6 us
    reduce_scatter x1, waiting for transfers between devices, on_device(): lax.psum_scatter(partials.astype(jnp.bfloat16), 'tp', scatter_dimension=0...  68.5 us
    all_gather x1, waiting for transfers between devices, on_device(): row_piece = lax.all_gather(arrived, 'tp', axis=0, tiled=True)  64.4 us
    another operation x2, other arithmetic  14.1 us
    all_gather x1, blocking collectives, on_device(): key_piece = lax.all_gather(keys, 'sp', axis=0, tiled=True)  13.4 us
    all_gather x1, blocking collectives, on_device(): value_piece = lax.all_gather(values, 'sp', axis=0, tiled=True)  12.4 us
    all_gather x1, blocking collectives, on_device(): bias_piece = lax.all_gather(key_bias, 'sp', axis=0, tiled=True)  11 us
    dot_general x1, matrix products, expert_partial(): jnp.dot(row_block, gate_matrix, preferred_element_type=jnp.float32)  9.96 us
  transfers between devices with their start and end apart: 8, of which 6 were waited for; matrix products, arithmetic and copies ran while one was open for 10% of the time, Pallas kernels for 0%

profile of v1, /device:TPU:0, one launch (start us, length us, event | category | flops | bytes accessed | tf_op | source)
XLA Modules:
  0.0 388.6 jit_solution(7817281751383652254)
XLA Ops:
  9.4 1.7 copy.81
  11.2 11.0 %all_gather.17 = bf16[1536,4]{0,1:T(4,128)(2,1)} all-gather(bf16[384,4]{0,1:T(4,128)(2,1)} %param.20), channel_id=1, replica_groups=mesh['sp'=4,'tp'=8] {'sp'}, dimensions={0}, use_global_device_ids=true | all-gather | bytes 15360 | tf_op jit(solution)/shard_map/all_gather | solution.py:121
  22.2 12.4 %all_gather.15 = bf16[1536,256]{0,1:T(8,128)(2,1)} all-gather(bf16[384,256]{0,1:T(8,128)(2,1)S(1)} %copy.79), channel_id=1, replica_groups=mesh['sp'=4,'tp'=8] {'sp'}, dimensions={0}, use_global_device_ids=true | all-gather | bytes 983040 | tf_op jit(solution)/shard_map/all_gather | solution.py:120
  34.5 13.4 %all_gather.16 = bf16[1536,256]{0,1:T(8,128)(2,1)} all-gather(bf16[384,256]{0,1:T(8,128)(2,1)S(1)} %copy.80), channel_id=1, replica_groups=mesh['sp'=4,'tp'=8] {'sp'}, dimensions={0}, use_global_device_ids=true | all-gather | bytes 983040 | tf_op jit(solution)/shard_map/all_gather | solution.py:119
  49.8 36.7 %while.17 = (s32[]{:T(128)}, f32[4,384,256]{1,2,0:T(8,128)}, f32[4,4,384]{2,1,0:T(4,128)}, s32[]{:T(128)}, bf16[1536,256]{0,1:T(8,128)(2,1)}, /*index=5*/bf16[15...) while((s32[]{:T(128)}, f32[4,384,256]{1,2,0:T(8,128)}, ...), condition=%wide.region_6.7_spmd.clone.clone, body=%wide.region_0.6_spmd.clone.clone.sunk | while | flops 246117120 | bytes 38572464 | solution.py:143
  49.8 28.0 %conditional.4 = ((f32[4,384,256]{1,2,0:T(8,128)}, f32[4,4,384]{2,1,0:T(4,128)})) conditional(s32[]{:T(128)} %convert_element_type.76, (f32[4,384,256]{1,2,0:T(8,128)}, f32[4,4,384]{2,1,0:T(4,128)}) %tuple.56, (s32[]{:T(128)}, bf16[1536,256]{0,1:T(8,128)(2,1)}, s32[]{:T(128)}, bf16[1536,256]{0,1:T(8,128)(2,1)}, bf16[384,4,64]{0,2,1:T(8,128)(2,1)}, ...), branch_computations={%region_1.0_spmd, %region_2.5_spmd} | conditional | flops 246117120 | bytes 38570716 | solution.py:141
  51.7 4.3 %fusion.15 = (f32[4,384]{1,0:T(4,128)S(1)}, f32[4,384,384]{1,2,0:T(8,128)S(1)}, f32[4,384,384]{2,1,0:T(8,128)}) fusion(f32[4,384]{1,0:T(4,128)S(1)} %convert_bitcast_fusion, pred[384,384]{0,1:T(8,128)(4,1)S(1)} %broadcast_compare_fusion, bf16[384,4,64]{0,2,1:T(8,128)(2,1)S(1)} %bitcast.103, bf16[384,4,64]{0,2,1:T(8,128)(2,1)} %get-tuple-element.177), kind=kOutput, calls=%fused_computation.34 | convolution fusion | flops 81984000 | bytes 5271552 | tf_op jit(solution)/shard_map/while/body/eval_jaxpr/cond/branch_1_fun/qhd,khd->hqk/dot_general | solution.py:92
  56.0 14.0 %fusion.2 = f32[4,384,3,128]{1,2,3,0:T(4,128)S(1)} fusion(f32[4,384,3,128]{1,3,2,0:T(8,128)S(1)} %bitcast.99), kind=kOutput, calls=%fused_computation.6 | output fusion | flops 74907648 | bytes 4718592 | tf_op jit(solution)/shard_map/reduce-window
  72.3 3.6 fusion.8
  91.8 4.8 %all-to-all-start = ((bf16[8,48,256]{2,1,0:T(8,128)(2,1)}), bf16[8,48,256]{2,1,0:T(8,128)(2,1)S(1)}, u32[]{:S(2)}, u32[]{:S(2)}) async-start(bf16[8,48,256]{2,1,0:T(8,128)(2,1)} %multiply_convert_fusion.2), calls=%async_computation | async-start | bytes 393216 | tf_op jit(solution)/shard_map/all_to_all | solution.py:155
  98.1 6.8 %all-to-all-done = bf16[8,48,256]{2,1,0:T(8,128)(2,1)S(1)} async-done(((bf16[8,48,256]{2,1,0:T(8,128)(2,1)}), bf16[8,48,256]{2,1,0:T(8,128)(2,1)S(1)}, u32[]{:S(2)}, u32[]{:S(2)}) %all-to-all-start) | async-done | bytes 196640 | tf_op jit(solution)/shard_map/all_to_all | solution.py:155
  104.9 5.1 %multiply_reduce_fusion.1 = (f32[48]{0:T(128)S(1)}, f32[48,2048]{1,0:T(8,128)S(1)}) fusion(bf16[48,2048]{1,0:T(8,128)(2,1)S(1)} %bitcast.105, bf16[2048,2048]{1,0:T(8,128)(2,1)} %all-gather.4.cloned.1.call-done, bf16[48,2048]{1,0:T(8,128)(2,1)S(1)} %copy-done.1), kind=kOutput, calls=%fused_computation.56 | convolution fusion | flops 403242944 | bytes 9175232 | tf_op jit(solution)/shard_map/dot_general | solution.py:156
  111.5 28.4 %collective-permute-start = (bf16[1,1,48,2048]{3,2,1,0:T(8,128)(2,1)S(1)}, bf16[1,1,48,2048]{3,2,1,0:T(8,128)(2,1)S(1)}, u32[]{:S(2)}, u32[]{:S(2)}) collective-permute-start(bf16[1,1,48,2048]{3,2,1,0:T(8,128)(2,1)S(1)} %get-tuple-element.272), channel_id=1, source_target_pairs={{0,8},{8,16},{16,24},{24,0},{1,9},{9,17},{17,25},{25,1},{2,10},{10... | collective-permute-start | bytes 589832 | tf_op jit(solution)/shard_map/ppermute | solution.py:29
  139.9 57.1 %collective-permute-start.1 = (bf16[1,1,48,2048]{3,2,1,0:T(8,128)(2,1)S(1)}, bf16[1,1,48,2048]{3,2,1,0:T(8,128)(2,1)S(1)}, u32[]{:S(2)}, u32[]{:S(2)}) collective-permute-start(bf16[1,1,48,2048]{3,2,1,0:T(8,128)(2,1)S(1)} %get-tuple-element.271), channel_id=1, source_target_pairs={{0,16},{8,24},{16,0},{24,8},{1,17},{9,25},{17,1},{25,9},{2,18},{10... | collective-permute-start | bytes 589832 | tf_op jit(solution)/shard_map/ppermute | solution.py:29
  197.1 5.2 %collective-permute-done = bf16[1,1,48,2048]{3,2,1,0:T(8,128)(2,1)S(1)} collective-permute-done((bf16[1,1,48,2048]{3,2,1,0:T(8,128)(2,1)S(1)}, bf16[1,1,48,2048]{3,2,1,0:T(8,128)(2,1)S(1)}, u32[]{:S(2)}, u32[]{:S(2)}) %collective-permute-start) | collective-permute-done | bytes 196640 | tf_op jit(solution)/shard_map/ppermute | solution.py:29
  202.3 2.2 collective-permute-done.1
  206.2 64.4 %all-gather.6.cloned.1.call-done = bf16[32,48,2048]{2,1,0:T(8,128)(2,1)} async-done(((bf16[4,48,2048]{2,1,0:T(8,128)(2,1)}), bf16[32,48,2048]{2,1,0:T(8,128)(2,1)}) %all-gather.6.cloned.1.call-update) | async-done | bytes 6291472 | tf_op jit(solution)/shard_map/all_gather | solution.py:172
  270.6 10.0 %fusion.18 = f32[1536,896]{1,0:T(8,128)S(1)} fusion(bf16[1536,2048]{1,0:T(8,128)(2,1)} %bitcast.115, bf16[1,2048,896]{2,1,0:T(8,128)(2,1)} %param.25), kind=kOutput, calls=%fused_computation.39 | convolution fusion | flops 5637144576 | bytes 15466496 | tf_op jit(solution)/shard_map/dot_general | solution.py:43
  280.6 7.1 %multiply_convert_fusion = bf16[1536,896]{1,0:T(8,128)(2,1)S(1)} fusion(f32[1536,896]{1,0:T(8,128)S(1)} %fusion.18, bf16[1536,2048]{1,0:T(8,128)(2,1)S(1)} %bitcast.116, bf16[1,2048,896]{2,1,0:T(8,128)(2,1)S(1)} %copy-done.7), kind=kOutput, calls=%fused_computation.36 | convolution fusion | flops 5645402112 | bytes 18219008 | tf_op jit(solution)/shard_map/dot_general | solution.py:44
  287.7 8.7 %convert_bitcast_fusion.1 = bf16[32,1,48,2048]{3,2,0,1:T(8,128)(2,1)} fusion(bf16[32,48,896]{2,1,0:T(8,128)(2,1)S(1)} %bitcast.117, bf16[1,896,2048]{2,1,0:T(8,128)(2,1)S(1)} %copy-done.8), kind=kOutput, calls=%fused_computation.35 | convolution fusion | flops 5640290304 | bytes 12713984 | tf_op jit(solution)/shard_map/dot_general | solution.py:46
  296.5 68.5 %reduce-scatter.2.cloned.1.call-done = bf16[4,1,48,2048]{3,2,0,1:T(8,128)(2,1)} async-done(((bf16[32,1,48,2048]{3,2,0,1:T(8,128)(2,1)}), bf16[4,1,48,2048]{3,2,0,1:T(8,128)(2,1)}) %reduce-scatter.2.cloned.1.call-update) | async-done | bytes 786448 | tf_op jit(solution)/shard_map/reduce_scatter | solution.py:182
  365.0 3.8 all-to-all-start.1
  369.3 8.7 %all-to-all-done.1 = bf16[4,1,48,2048]{3,2,1,0:T(8,128)(2,1)S(1)} async-done(((bf16[4,1,48,2048]{3,2,1,0:T(8,128)(2,1)}), bf16[4,1,48,2048]{3,2,1,0:T(8,128)(2,1)S(1)}, u32[]{:S(2)}, u32[]{:S(2)}) %all-to-all-start.1) | async-done | bytes 786464 | tf_op jit(solution)/shard_map/all_to_all | solution.py:183
  379.0 2.1 multiply_reduce_fusion
  (98 shorter events, 22.8 us)
Async XLA Ops:
  6.5 98.4 %all-gather.4.cloned.1.call-start = ((), (), s32[]{:S(2)}) async-start(), calls=%async_computation.3 | async-start | bytes 9437184 | tf_op jit(solution)/shard_map/all_gather | solution.py:158
  70.6 1.7 copy-start
  88.0 3.0 copy-start.4
  89.6 7.0 %copy-start.3 = (s32[48,2]{0,1:T(2,128)S(1)}, s32[48,2]{0,1:T(2,128)}, u32[]{:S(2)}) copy-start(s32[48,2]{0,1:T(2,128)} %param.28) | copy-start | bytes 1156
  89.8 15.1 %copy-start.1 = (bf16[48,2048]{1,0:T(8,128)(2,1)S(1)}, bf16[48,2048]{1,0:T(8,128)(2,1)}, u32[]{:S(2)}) copy-start(bf16[48,2048]{1,0:T(8,128)(2,1)} %param.23) | copy-start | bytes 589828
  91.8 13.1 %all-to-all-start = ((bf16[8,48,256]{2,1,0:T(8,128)(2,1)}), bf16[8,48,256]{2,1,0:T(8,128)(2,1)S(1)}, u32[]{:S(2)}, u32[]{:S(2)}) async-start(bf16[8,48,256]{2,1,0:T(8,128)(2,1)} %multiply_convert_fusion.2), calls=%async_computation | async-start | bytes 393216 | tf_op jit(solution)/shard_map/all_to_all | solution.py:155
  96.5 174.1 %all-gather.6.cloned.1.call-start = ((), (), s32[]{:S(2)}) async-start(), calls=%async_computation.5 | async-start | bytes 7077888 | tf_op jit(solution)/shard_map/all_gather | solution.py:172
  104.9 5.1 %copy-start.2 = (f32[2048]{0:T(1024)S(1)}, f32[2048]{0:T(1024)}, u32[]{:S(2)}) copy-start(f32[2048]{0:T(1024)} %param.24) | copy-start | bytes 24580
  111.5 90.8 %collective-permute-start = (bf16[1,1,48,2048]{3,2,1,0:T(8,128)(2,1)S(1)}, bf16[1,1,48,2048]{3,2,1,0:T(8,128)(2,1)S(1)}, u32[]{:S(2)}, u32[]{:S(2)}) collective-permute-start(bf16[1,1,48,2048]{3,2,1,0:T(8,128)(2,1)S(1)} %get-tuple-element.272), channel_id=1, source_target_pairs={{0,8},{8,16},{16,24},{24,0},{1,9},{9,17},{17,25},{25,1},{2,10},{10... | collective-permute-start | bytes 589832 | tf_op jit(solution)/shard_map/ppermute | solution.py:29
  139.9 64.6 %collective-permute-start.1 = (bf16[1,1,48,2048]{3,2,1,0:T(8,128)(2,1)S(1)}, bf16[1,1,48,2048]{3,2,1,0:T(8,128)(2,1)S(1)}, u32[]{:S(2)}, u32[]{:S(2)}) collective-permute-start(bf16[1,1,48,2048]{3,2,1,0:T(8,128)(2,1)S(1)} %get-tuple-element.271), channel_id=1, source_target_pairs={{0,16},{8,24},{16,0},{24,8},{1,17},{9,25},{17,1},{25,9},{2,18},{10... | collective-permute-start | bytes 589832 | tf_op jit(solution)/shard_map/ppermute | solution.py:29
  197.0 7.4 %collective-permute-start.2 = (bf16[1,1,48,2048]{3,2,1,0:T(8,128)(2,1)S(1)}, bf16[1,1,48,2048]{3,2,1,0:T(8,128)(2,1)S(1)}, u32[]{:S(2)}, u32[]{:S(2)}) collective-permute-start(bf16[1,1,48,2048]{3,2,1,0:T(8,128)(2,1)S(1)} %get-tuple-element.270), channel_id=1, source_target_pairs={{0,24},{8,0},{16,8},{24,16},{1,25},{9,1},{17,9},{25,17},{2,26},{10... | collective-permute-start | bytes 589832 | tf_op jit(solution)/shard_map/ppermute | solution.py:29
  206.1 158.9 %reduce-scatter.2.cloned.1.call-start = ((), (), s32[]{:S(2)}) async-start(), calls=%async_computation.4 | async-start | bytes 7077888 | tf_op jit(solution)/shard_map/reduce_scatter | solution.py:182
  270.6 10.0 %copy-start.6 = (bf16[32,48,2048]{2,1,0:T(8,128)(2,1)S(1)}, bf16[32,48,2048]{2,1,0:T(8,128)(2,1)}, u32[]{:S(2)}) copy-start(bf16[32,48,2048]{2,1,0:T(8,128)(2,1)} %all-gather.6.cloned.1.call-done) | copy-start | bytes 18874372
  270.6 10.0 %copy-start.7 = (bf16[1,2048,896]{2,1,0:T(8,128)(2,1)S(1)}, bf16[1,2048,896]{2,1,0:T(8,128)(2,1)}, u32[]{:S(2)}) copy-start(bf16[1,2048,896]{2,1,0:T(8,128)(2,1)} %param.26) | copy-start | bytes 11010052
  280.6 7.1 %copy-start.8 = (bf16[1,896,2048]{2,1,0:T(8,128)(2,1)S(1)}, bf16[1,896,2048]{2,1,0:T(8,128)(2,1)}, u32[]{:S(2)}) copy-start(bf16[1,896,2048]{2,1,0:T(8,128)(2,1)} %param.27) | copy-start | bytes 11010052
  296.4 72.7 %copy-start.5 = (f32[48,2]{0,1:T(2,128)S(1)}, f32[48,2]{0,1:T(2,128)}, u32[]{:S(2)}) copy-start(f32[48,2]{0,1:T(2,128)} %param.29) | copy-start | bytes 1156
  365.0 12.9 %all-to-all-start.1 = ((bf16[4,1,48,2048]{3,2,1,0:T(8,128)(2,1)}), bf16[4,1,48,2048]{3,2,1,0:T(8,128)(2,1)S(1)}, u32[]{:S(2)}, u32[]{:S(2)}) async-start(bf16[4,1,48,2048]{3,2,1,0:T(8,128)(2,1)} %bitcast.107), calls=%async_computation.2 | async-start | bytes 1572864 | tf_op jit(solution)/shard_map/all_to_all | solution.py:183
Sparse Core Ops, SparseCore 0:
  8.9 84.7 all-gather.3
  206.2 64.3 all-gather.5
  296.6 68.3 reduce-scatter.1
